TPU v7x, 32 devices: a whole 2x2x4 slice. The times are simulated.
32 devices in a mesh: fs: 8 (over z, y), tp: 4 (over x, core).
Axes of the slice: x: 2, y: 2, z: 4, core: 2. Of those that a mesh axis runs over, the one named last changes fastest.
Arguments:
- tokens: bfloat16 [6144, 2048], P(('fs', 'tp')), may hold values from -60 to 60
- norm_gain: float32 [2048], P('fs'), may hold values from 0.1 to 1.9
- gate_weight: float32 [2048, 5632], P('fs', 'tp'), may hold values from -0.125 to 0.125
- up_weight: float32 [2048, 5632], P('fs', 'tp'), may hold values from -0.125 to 0.125
- down_weight: float32 [2048, 5632], P('fs', 'tp'), may hold values from -0.078125 to 0.078125
Outputs:
- mixed_rows: bfloat16 [6144, 2048], P(('fs', 'tp'))
- gate_out: bfloat16 [2048, 5632], P(None, 'tp')
- up_out: bfloat16 [2048, 5632], P(None, 'tp')
- down_out: bfloat16 [2048, 5632], P(None, 'tp')
All inputs are finite; a program needn't handle non-finite values.
Results may differ from a plain program's by a relative error of at most 0.014.
Values may be sent and summed in bfloat16 or wider, within the bound.
A program may use at most 128 MiB of HBM per device.

v0:
```python
import jax
import jax.numpy as jnp
from jax import lax
from jax.sharding import PartitionSpec as P


def normalize(source):
    widened = source.astype(jnp.float32)
    return (widened * lax.rsqrt(jnp.mean(widened * widened, axis=1, keepdims=True) + 1e-06)).astype(
        jnp.bfloat16
    )


def shards(tokens, norm_gain, gate_weight, up_weight, down_weight):
    row_gain = norm_gain[:, None]
    gate_local = (gate_weight * row_gain).astype(jnp.bfloat16)
    up_local = (up_weight * row_gain).astype(jnp.bfloat16)
    down_local = down_weight.astype(jnp.bfloat16)
    normed = normalize(tokens)
    gathered = lax.all_gather(normed, "tp", axis=0, tiled=True)
    down_whole = lax.all_gather(down_local, "fs", axis=0, tiled=True)
    gate_piece = lax.all_gather(gate_local, "fs", axis=0, tiled=True)
    up_piece = lax.all_gather(up_local, "fs", axis=0, tiled=True)
    gate_acc = jnp.dot(gathered, gate_piece, preferred_element_type=jnp.float32)
    up_acc = jnp.dot(gathered, up_piece, preferred_element_type=jnp.float32)
    hidden = (jax.nn.silu(gate_acc) * up_acc).astype(jnp.bfloat16)
    partial_value = lax.dot_general(
        hidden, down_whole, (((1,), (1,)), ((), ())), preferred_element_type=jnp.float32
    )
    mixed_rows = lax.psum_scatter(
        lax.optimization_barrier(partial_value.astype(jnp.bfloat16))
        .astype(jnp.float32)
        .astype(jnp.bfloat16),
        "tp",
        scatter_dimension=0,
        tiled=True,
    )
    return (mixed_rows, gate_piece, up_piece, down_whole)


def solution(mesh):
    in_specs = (P(("fs", "tp"), None), P("fs"), P("fs", "tp"), P("fs", "tp"), P("fs", "tp"))
    out_specs = (P(("fs", "tp"), None), P(None, "tp"), P(None, "tp"), P(None, "tp"))
    return jax.shard_map(shards, mesh=mesh, in_specs=in_specs, out_specs=out_specs, check_vma=False)
```

profile of v0, /device:TPU:0, one launch (start us, length us, event | category | flops | bytes accessed | tf_op | source)
XLA Modules:
  0.0 397.9 jit_solution(9030108663980922372)
XLA Ops:
  7.2 0.0 copy-start
  7.2 0.0 all-gather.5.cloned.1.call-start
  7.2 1.5 fusion
  8.7 2.2 fusion.1
  10.9 0.0 all-gather.5.cloned.1.call-update
  10.9 0.0 all-gather.7.cloned.1.call-start
  11.0 3.2 multiply_convert_fusion.1
  14.2 0.0 all-gather.7.cloned.1.call-update
  14.2 0.0 all-gather.11.cloned.1.call-start
  14.2 0.0 copy-done
  14.2 0.9 convert_element_type.28
  15.2 0.0 all-gather.11.cloned.1.call-update
  15.2 0.0 all-gather.9.cloned.1.call-start
  15.3 0.5 all-gather.9.cloned.1.call-update
  15.8 0.0 reduce-scatter.2.cloned.1.call-start
  15.8 26.5 %all-gather.5.cloned.1.call-done = bf16[768,2048]{1,0:T(8,128)(2,1)} async-done(((bf16[192,2048]{1,0:T(8,128)(2,1)}), bf16[768,2048]{1,0:T(8,128)(2,1)}) %all-gather.5.cloned.1.call-update) | async-done | bytes 3145744 | tf_op jit(solution)/shard_map/all_gather | solution.py:20
  42.3 0.0 copy-start.1
  42.3 95.1 %all-gather.7.cloned.1.call-done = bf16[2048,1408]{1,0:T(8,128)(2,1)} async-done(((bf16[256,1408]{1,0:T(8,128)(2,1)}), bf16[2048,1408]{1,0:T(8,128)(2,1)}) %all-gather.7.cloned.1.call-update) | async-done | bytes 5767184 | tf_op jit(solution)/shard_map/all_gather | solution.py:22
  137.4 9.7 %fusion.3 = f32[768,1408]{1,0:T(8,128)} fusion(bf16[768,2048]{1,0:T(8,128)(2,1)} %all-gather.5.cloned.1.call-done, bf16[2048,1408]{1,0:T(8,128)(2,1)} %all-gather.7.cloned.1.call-done), kind=kOutput, calls=%fused_computation.10 | convolution fusion | flops 4429185024 | bytes 13238272 | tf_op jit(solution)/shard_map/dot_general | solution.py:24
  147.1 83.6 %all-gather.11.cloned.1.call-done = bf16[2048,1408]{1,0:T(8,128)(2,1)} async-done(((bf16[256,1408]{1,0:T(8,128)(2,1)}), bf16[2048,1408]{1,0:T(8,128)(2,1)}) %all-gather.11.cloned.1.call-update) | async-done | bytes 5767184 | tf_op jit(solution)/shard_map/all_gather | solution.py:21
  230.7 93.1 %all-gather.9.cloned.1.call-done = bf16[2048,1408]{1,0:T(8,128)(2,1)} async-done(((bf16[256,1408]{1,0:T(8,128)(2,1)}), bf16[2048,1408]{1,0:T(8,128)(2,1)}) %all-gather.9.cloned.1.call-update) | async-done | bytes 5767184 | tf_op jit(solution)/shard_map/all_gather | solution.py:23
  323.8 0.0 copy-done.1
  323.8 17.3 %convolution_convert_fusion = bf16[768,2048]{1,0:T(8,128)(2,1)} fusion(bf16[2048,1408]{1,0:T(8,128)(2,1)} %all-gather.11.cloned.1.call-done, f32[768,1408]{1,0:T(8,128)} %fusion.3, bf16[768,2048]{1,0:T(8,128)(2,1)S(1)} %copy-done.1, bf16[2048,1408]{1,0:T(8,128)(2,1)} %all-gather.9.cloned.1.call-done), kind=kOutput, calls=%fused_computation.1 | convolution fusion | flops 8866430976 | bytes 22151168 | tf_op jit(solution)/shard_map/dot_general | solution.py:27
  341.2 0.0 reduce-scatter.2.cloned.1.call-update
  341.2 36.2 %reduce-scatter.2.cloned.1.call-done = bf16[192,2048]{1,0:T(8,128)(2,1)} async-done(((bf16[768,2048]{1,0:T(8,128)(2,1)}), bf16[192,2048]{1,0:T(8,128)(2,1)}) %reduce-scatter.2.cloned.1.call-update) | async-done | bytes 786448 | tf_op jit(solution)/shard_map/reduce_scatter | solution.py:30
  377.4 0.0 slice-start
  377.4 5.7 %copy.12 = bf16[2048,1408]{1,0:T(8,128)(2,1)} copy(bf16[2048,1408]{1,0:T(8,128)(2,1)} %all-gather.7.cloned.1.call-done) | data formatting | bytes 11534336
  383.2 0.0 slice-start.1
  383.2 5.7 %copy.13 = bf16[2048,1408]{1,0:T(8,128)(2,1)} copy(bf16[2048,1408]{1,0:T(8,128)(2,1)} %all-gather.9.cloned.1.call-done) | data formatting | bytes 11534336
  388.9 0.0 slice-done
  388.9 0.0 slice-done.1
  388.9 2.5 copy.14
  (2 shorter events, 0.0 us)
Async XLA Ops:
  7.2 7.1 %copy-start = (f32[256,1408]{1,0:T(8,128)S(1)}, f32[256,1408]{1,0:T(8,128)}, u32[]{:S(2)}) copy-start(f32[256,1408]{1,0:T(8,128)} %param.9) | copy-start | bytes 4325380
  7.2 35.2 %all-gather.5.cloned.1.call-start = ((), (), s32[]{:S(2)}) async-start(), calls=%async_computation.1 | async-start | bytes 3932160 | tf_op jit(solution)/shard_map/all_gather | solution.py:20
  10.9 126.5 %all-gather.7.cloned.1.call-start = ((), (), s32[]{:S(2)}) async-start(), calls=%async_computation.2 | async-start | bytes 6488064 | tf_op jit(solution)/shard_map/all_gather | solution.py:22
  14.2 216.5 %all-gather.11.cloned.1.call-start = ((), (), s32[]{:S(2)}) async-start(), calls=%async_computation.4 | async-start | bytes 6488064 | tf_op jit(solution)/shard_map/all_gather | solution.py:21
  15.2 308.6 %all-gather.9.cloned.1.call-start = ((), (), s32[]{:S(2)}) async-start(), calls=%async_computation.3 | async-start | bytes 6488064 | tf_op jit(solution)/shard_map/all_gather | solution.py:23
  15.8 361.6 %reduce-scatter.2.cloned.1.call-start = ((), (), s32[]{:S(2)}) async-start(), calls=%async_computation.5 | async-start | bytes 3932160 | tf_op jit(solution)/shard_map/reduce_scatter | solution.py:30
  42.3 281.5 %copy-start.1 = (bf16[768,2048]{1,0:T(8,128)(2,1)S(1)}, bf16[768,2048]{1,0:T(8,128)(2,1)}, u32[]{:S(2)}) copy-start(bf16[768,2048]{1,0:T(8,128)(2,1)} %all-gather.5.cloned.1.call-done) | copy-start | bytes 9437188
  377.4 11.5 %slice-start = ((s8[5767168]{0:T(1024)(128)(4,1)}), s8[4194304]{0:T(1024)(128)(4,1)S(1)}, s32[]{:S(2)}) async-start(s8[5767168]{0:T(1024)(128)(4,1)} %bitcast.5), calls=%async_computation.6 | async-start | bytes 8388608
  383.2 5.7 %slice-start.1 = ((s8[5767168]{0:T(1024)(128)(4,1)}), s8[1572864]{0:T(1024)(128)(4,1)S(1)}, s32[]{:S(2)}) async-start(s8[5767168]{0:T(1024)(128)(4,1)} %bitcast.5), calls=%async_computation.7 | async-start | bytes 3145728
Sparse Core Ops, SparseCore 0:
  11.1 31.2 all-gather.4
  45.1 92.2 all-gather.6
  140.2 90.4 all-gather.10
  233.3 90.4 all-gather.8
  341.3 36.0 reduce-scatter.1
where the time goes:
time: 398 us
  waiting for transfers between devices  335 us (84%)
  matrix products  27 us (7%)
  local copies, waits for them, and re-layouts  14 us (4%)
  between operations  13.8 us (3%)
  other arithmetic  7.8 us (2%)
    all_gather x1, waiting for transfers between devices, shards(): gate_piece = lax.all_gather(gate_local, 'fs', axis=0, tiled=True)  95.1 us
    all_gather x1, waiting for transfers between devices, shards(): up_piece = lax.all_gather(up_local, 'fs', axis=0, tiled=True)  93.1 us
    all_gather x1, waiting for transfers between devices, shards(): down_whole = lax.all_gather(down_local, 'fs', axis=0, tiled=True)  83.6 us
    reduce_scatter x1, waiting for transfers between devices, shards(): lax.psum_scatter(lax.optimization_barrier(partial_value.astype(jnp.bfloat...  36.2 us
    all_gather x1, waiting for transfers between devices, shards(): gathered = lax.all_gather(normed, 'tp', axis=0, tiled=True)  26.5 us
    dot_general x1, matrix products, shards(): lax.dot_general(hidden, down_whole, (((1,), (1,)), ((), ())), preferred_e...  17.3 us
    unnamed x11, local copies, waits for them, and re-layouts  14 us
    dot_general x1, matrix products, shards(): gate_acc = jnp.dot(gathered, gate_piece, preferred_element_type=jnp.float32)  9.67 us
  transfers between devices with their start and end apart: 5, of which 5 were waited for; matrix products, arithmetic and copies ran while one was open for 3% of the time, Pallas kernels for 0%

commit v1 on v0

--- a/solution.py
+++ b/solution.py
@@ -20,7 +20,12 @@
     gathered = lax.all_gather(normed, "tp", axis=0, tiled=True)
     down_whole = lax.all_gather(down_local, "fs", axis=0, tiled=True)
     gate_piece = lax.all_gather(gate_local, "fs", axis=0, tiled=True)
-    up_piece = lax.all_gather(up_local, "fs", axis=0, tiled=True)
+    ring = [up_local]
+    for hop in range(7):
+        ring.append(lax.ppermute(ring[-1], "fs", [(dev, (dev + 1) % 8) for dev in range(8)]))
+    up_piece = jnp.roll(
+        jnp.concatenate(ring[::-1], axis=0), (lax.axis_index("fs") + 1) * ring[0].shape[0], axis=0
+    )
     gate_acc = jnp.dot(gathered, gate_piece, preferred_element_type=jnp.float32)
     up_acc = jnp.dot(gathered, up_piece, preferred_element_type=jnp.float32)
     hidden = (jax.nn.silu(gate_acc) * up_acc).astype(jnp.bfloat16)

time: 398 us -> 357 us (0.90)
  waiting for transfers between devices: 335 us -> 280 us
  local copies, waits for them, and re-layouts: 14 us -> 24.1 us
    ppermute x0 -> x7, waiting for transfers between devices: none -> 193 us  [shards(): lax.ppermute(ring[-1], 'fs', [(dev, (dev + 1) % 8) for dev in range(8)])]
    all_gather x1, waiting for transfers between devices: 95.1 us -> 0.01 us  [shards(): gate_piece = lax.all_gather(gate_local, 'fs', axis=0, tiled=True)]
    all_gather x1 -> x0, waiting for transfers between devices: 93.1 us -> none  [shards(): up_piece = lax.all_gather(up_local, 'fs', axis=0, tiled=True)]
    all_gather x1, waiting for transfers between devices: 83.6 us -> 50.6 us  [shards(): down_whole = lax.all_gather(down_local, 'fs', axis=0, tiled=True)]
    all_gather x1, waiting for transfers between devices: 26.5 us -> 0.01 us  [shards(): gathered = lax.all_gather(normed, 'tp', axis=0, tiled=True)]
    unnamed x11 -> x25, local copies, waits for them, and re-layouts: 14 us -> 21 us
  transfers between devices with their start and end apart: 5 -> 11, of which waited for: 5 -> 9; matrix products, arithmetic and copies ran while one was open for 3% -> 7% of each run, Pallas kernels for 0% -> 0%
where the time goes in v1:
time: 357 us
  waiting for transfers between devices  280 us (78%)
  matrix products  26.4 us (7%)
  local copies, waits for them, and re-layouts  24.1 us (7%)
  between operations  13.9 us (4%)
  other arithmetic  8.82 us (2%)
    ppermute x7, waiting for transfers between devices, shards(): lax.ppermute(ring[-1], 'fs', [(dev, (dev + 1) % 8) for dev in range(8)])  193 us
    all_gather x1, waiting for transfers between devices, shards(): down_whole = lax.all_gather(down_local, 'fs', axis=0, tiled=True)  50.6 us
    reduce_scatter x1, waiting for transfers between devices, shards(): lax.psum_scatter(lax.optimization_barrier(partial_value.astype(jnp.bfloat...  36.2 us
    unnamed x25, local copies, waits for them, and re-layouts  21 us
    dot_general x1, matrix products, shards(): lax.dot_general(hidden, down_whole, (((1,), (1,)), ((), ())), preferred_e...  16.7 us
    dot_general x1, matrix products, shards(): gate_acc = jnp.dot(gathered, gate_piece, preferred_element_type=jnp.float32)  9.67 us
  transfers between devices with their start and end apart: 11, of which 9 were waited for; matrix products, arithmetic and copies ran while one was open for 7% of the time, Pallas kernels for 0%

profile of v1, /device:TPU:0, one launch (start us, length us, event | category | flops | bytes accessed | tf_op | source)
XLA Modules:
  0.0 356.7 jit_solution(11975395129454846170)
XLA Ops:
  7.2 0.0 all-gather.4.cloned.1.call-start
  7.2 1.4 fusion
  8.6 2.2 fusion.1
  10.8 0.0 all-gather.4.cloned.1.call-update
  10.8 0.0 all-gather.6.cloned.1.call-start
  10.9 2.9 multiply_convert_fusion.1
  13.8 0.0 all-gather.6.cloned.1.call-update
  13.8 0.0 all-gather.8.cloned.1.call-start
  13.9 3.0 collective-permute-start
  16.9 19.2 %collective-permute-done = bf16[256,1408]{1,0:T(8,128)(2,1)S(1)} collective-permute-done((bf16[256,1408]{1,0:T(8,128)(2,1)S(1)}, bf16[256,1408]{1,0:T(8,128)(2,1)S(1)}, u32[]{:S(2)}, u32[]{:S(2)}) %collective-permute-start) | collective-permute-done | bytes 720928 | tf_op jit(solution)/shard_map/ppermute | solution.py:25
  36.1 0.0 collective-permute-start.1
  36.1 2.3 convert_element_type.28
  38.4 0.0 all-gather.8.cloned.1.call-update
  38.4 0.0 reduce-scatter.2.cloned.1.call-start
  38.5 17.7 %collective-permute-done.1 = bf16[256,1408]{1,0:T(8,128)(2,1)S(1)} collective-permute-done((bf16[256,1408]{1,0:T(8,128)(2,1)S(1)}, bf16[256,1408]{1,0:T(8,128)(2,1)S(1)}, u32[]{:S(2)}, u32[]{:S(2)}) %collective-permute-start.1) | collective-permute-done | bytes 720928 | tf_op jit(solution)/shard_map/ppermute | solution.py:25
  56.1 0.0 collective-permute-start.2
  56.1 36.2 %collective-permute-done.2 = bf16[256,1408]{1,0:T(8,128)(2,1)S(1)} collective-permute-done((bf16[256,1408]{1,0:T(8,128)(2,1)S(1)}, bf16[256,1408]{1,0:T(8,128)(2,1)S(1)}, u32[]{:S(2)}, u32[]{:S(2)}) %collective-permute-start.2) | collective-permute-done | bytes 720928 | tf_op jit(solution)/shard_map/ppermute | solution.py:25
  92.4 0.0 collective-permute-start.3
  92.4 26.3 %collective-permute-done.3 = bf16[256,1408]{1,0:T(8,128)(2,1)S(1)} collective-permute-done((bf16[256,1408]{1,0:T(8,128)(2,1)S(1)}, bf16[256,1408]{1,0:T(8,128)(2,1)S(1)}, u32[]{:S(2)}, u32[]{:S(2)}) %collective-permute-start.3) | collective-permute-done | bytes 720928 | tf_op jit(solution)/shard_map/ppermute | solution.py:25
  118.6 0.0 copy-start
  118.6 0.9 copy-done
  119.5 0.0 collective-permute-start.4
  119.5 35.7 %collective-permute-done.4 = bf16[256,1408]{1,0:T(8,128)(2,1)S(1)} collective-permute-done((bf16[256,1408]{1,0:T(8,128)(2,1)S(1)}, bf16[256,1408]{1,0:T(8,128)(2,1)S(1)}, u32[]{:S(2)}, u32[]{:S(2)}) %collective-permute-start.4) | collective-permute-done | bytes 720928 | tf_op jit(solution)/shard_map/ppermute | solution.py:25
  155.2 0.0 copy-start.2
  155.2 0.9 copy-done.2
  156.1 0.0 collective-permute-start.5
  156.1 34.4 %collective-permute-done.5 = bf16[256,1408]{1,0:T(8,128)(2,1)} collective-permute-done((bf16[256,1408]{1,0:T(8,128)(2,1)S(1)}, bf16[256,1408]{1,0:T(8,128)(2,1)}, u32[]{:S(2)}, u32[]{:S(2)}) %collective-permute-start.5) | collective-permute-done | bytes 720928 | tf_op jit(solution)/shard_map/ppermute | solution.py:25
  190.4 0.0 collective-permute-start.6
  190.4 24.0 %collective-permute-done.6 = bf16[256,1408]{1,0:T(8,128)(2,1)} collective-permute-done((bf16[256,1408]{1,0:T(8,128)(2,1)}, bf16[256,1408]{1,0:T(8,128)(2,1)}, u32[]{:S(2)}, u32[]{:S(2)}) %collective-permute-start.6) | collective-permute-done | bytes 720928 | tf_op jit(solution)/shard_map/ppermute | solution.py:25
  214.5 1.2 constant_dynamic-update-slice_fusion.15
  215.6 1.2 constant_dynamic-update-slice_fusion.14
  216.8 0.0 copy-start.3
  216.9 1.3 constant_dynamic-update-slice_fusion.13
  218.1 0.0 copy-start.1
  218.1 1.3 constant_dynamic-update-slice_fusion.12
  219.4 0.1 constant_dynamic-update-slice_fusion.11
  219.5 0.1 constant_dynamic-update-slice_fusion.10
  219.6 0.1 constant_dynamic-update-slice_fusion.9
  219.7 0.1 constant_dynamic-update-slice_fusion.8
  219.8 1.2 constant_dynamic-update-slice_fusion.7
  221.0 1.2 constant_dynamic-update-slice_fusion.6
  222.2 0.0 copy-done.3
  222.2 0.1 constant_dynamic-update-slice_fusion.5
  222.3 0.0 copy-done.1
  222.3 0.1 constant_dynamic-update-slice_fusion.4
  222.4 0.1 constant_dynamic-update-slice_fusion.3
  222.5 0.1 constant_dynamic-update-slice_fusion.2
  222.6 0.1 constant_dynamic-update-slice_fusion.1
  222.7 0.1 constant_dynamic-update-slice_fusion
  222.8 3.0 constant_dynamic-slice_fusion
  225.8 0.0 all-gather.4.cloned.1.call-done
  225.8 0.0 all-gather.6.cloned.1.call-done
  225.8 9.7 %fusion.3 = f32[768,1408]{1,0:T(8,128)} fusion(bf16[768,2048]{1,0:T(8,128)(2,1)} %all-gather.4.cloned.1.call-done, bf16[2048,1408]{1,0:T(8,128)(2,1)} %all-gather.6.cloned.1.call-done), kind=kOutput, calls=%fused_computation.27 | convolution fusion | flops 4429185024 | bytes 13238272 | tf_op jit(solution)/shard_map/dot_general | solution.py:29
  235.4 50.6 %all-gather.8.cloned.1.call-done = bf16[2048,1408]{1,0:T(8,128)(2,1)} async-done(((bf16[256,1408]{1,0:T(8,128)(2,1)}), bf16[2048,1408]{1,0:T(8,128)(2,1)}) %all-gather.8.cloned.1.call-update) | async-done | bytes 5767184 | tf_op jit(solution)/shard_map/all_gather | solution.py:21
  286.1 16.7 %convolution_convert_fusion = bf16[768,2048]{1,0:T(8,128)(2,1)} fusion(bf16[2048,1408]{1,0:T(8,128)(2,1)} %all-gather.8.cloned.1.call-done, f32[768,1408]{1,0:T(8,128)} %fusion.3, bf16[768,2048]{1,0:T(8,128)(2,1)} %all-gather.4.cloned.1.call-done, bf16[2048,1408]{1,0:T(8,128)(2,1)} %constant_dynamic-slice_fusion), kind=kOutput, calls=%fused_computation.1 | convolution fusion | flops 8866430976 | bytes 22151168 | tf_op jit(solution)/shard_map/dot_general | solution.py:32
  302.8 0.0 reduce-scatter.2.cloned.1.call-update
  302.8 36.2 %reduce-scatter.2.cloned.1.call-done = bf16[192,2048]{1,0:T(8,128)(2,1)} async-done(((bf16[768,2048]{1,0:T(8,128)(2,1)}), bf16[192,2048]{1,0:T(8,128)(2,1)}) %reduce-scatter.2.cloned.1.call-update) | async-done | bytes 786448 | tf_op jit(solution)/shard_map/reduce_scatter | solution.py:35
  339.0 5.6 %copy.26 = bf16[2048,1408]{1,0:T(8,128)(2,1)} copy(bf16[2048,1408]{1,0:T(8,128)(2,1)} %all-gather.6.cloned.1.call-done) | data formatting | bytes 11534336
  344.6 5.6 %copy.27 = bf16[2048,1408]{1,0:T(8,128)(2,1)} copy(bf16[2048,1408]{1,0:T(8,128)(2,1)} %all-gather.8.cloned.1.call-done) | data formatting | bytes 11534336
  (1 shorter events, 0.0 us)
Async XLA Ops:
  7.2 218.6 %all-gather.4.cloned.1.call-start = ((), (), s32[]{:S(2)}) async-start(), calls=%async_computation.1 | async-start | bytes 3932160 | tf_op jit(solution)/shard_map/all_gather | solution.py:20
  10.8 214.9 %all-gather.6.cloned.1.call-start = ((), (), s32[]{:S(2)}) async-start(), calls=%async_computation.2 | async-start | bytes 6488064 | tf_op jit(solution)/shard_map/all_gather | solution.py:22
  13.8 272.2 %all-gather.8.cloned.1.call-start = ((), (), s32[]{:S(2)}) async-start(), calls=%async_computation.3 | async-start | bytes 6488064 | tf_op jit(solution)/shard_map/all_gather | solution.py:21
  13.9 22.2 %collective-permute-start = (bf16[256,1408]{1,0:T(8,128)(2,1)S(1)}, bf16[256,1408]{1,0:T(8,128)(2,1)S(1)}, u32[]{:S(2)}, u32[]{:S(2)}) collective-permute-start(bf16[256,1408]{1,0:T(8,128)(2,1)S(1)} %get-tuple-element.4), channel_id=1, source_target_pairs={{0,4},{4,8},{8,12},{12,16},{16,20},{20,24},{24,28},{28,0},{1,5},{5... | collective-permute-start | bytes 2162696 | tf_op jit(solution)/shard_map/ppermute | solution.py:25
  36.1 20.0 %collective-permute-start.1 = (bf16[256,1408]{1,0:T(8,128)(2,1)S(1)}, bf16[256,1408]{1,0:T(8,128)(2,1)S(1)}, u32[]{:S(2)}, u32[]{:S(2)}) collective-permute-start(bf16[256,1408]{1,0:T(8,128)(2,1)S(1)} %collective-permute-done), channel_id=1, source_target_pairs={{0,4},{4,8},{8,12},{12,16},{16,20},{20,24},{24,28},{28,0},{1,5},{5... | collective-permute-start | bytes 2162696 | tf_op jit(solution)/shard_map/ppermute | solution.py:25
  38.4 300.6 %reduce-scatter.2.cloned.1.call-start = ((), (), s32[]{:S(2)}) async-start(), calls=%async_computation.4 | async-start | bytes 3932160 | tf_op jit(solution)/shard_map/reduce_scatter | solution.py:35
  56.1 36.2 %collective-permute-start.2 = (bf16[256,1408]{1,0:T(8,128)(2,1)S(1)}, bf16[256,1408]{1,0:T(8,128)(2,1)S(1)}, u32[]{:S(2)}, u32[]{:S(2)}) collective-permute-start(bf16[256,1408]{1,0:T(8,128)(2,1)S(1)} %collective-permute-done.1), channel_id=1, source_target_pairs={{0,4},{4,8},{8,12},{12,16},{16,20},{20,24},{24,28},{28,0},{1,5},{5... | collective-permute-start | bytes 2162696 | tf_op jit(solution)/shard_map/ppermute | solution.py:25
  92.4 26.3 %collective-permute-start.3 = (bf16[256,1408]{1,0:T(8,128)(2,1)S(1)}, bf16[256,1408]{1,0:T(8,128)(2,1)S(1)}, u32[]{:S(2)}, u32[]{:S(2)}) collective-permute-start(bf16[256,1408]{1,0:T(8,128)(2,1)S(1)} %collective-permute-done.2), channel_id=1, source_target_pairs={{0,4},{4,8},{8,12},{12,16},{16,20},{20,24},{24,28},{28,0},{1,5},{5... | collective-permute-start | bytes 2162696 | tf_op jit(solution)/shard_map/ppermute | solution.py:25
  118.6 0.9 copy-start
  119.5 35.7 %collective-permute-start.4 = (bf16[256,1408]{1,0:T(8,128)(2,1)S(1)}, bf16[256,1408]{1,0:T(8,128)(2,1)S(1)}, u32[]{:S(2)}, u32[]{:S(2)}) collective-permute-start(bf16[256,1408]{1,0:T(8,128)(2,1)S(1)} %collective-permute-done.3), channel_id=1, source_target_pairs={{0,4},{4,8},{8,12},{12,16},{16,20},{20,24},{24,28},{28,0},{1,5},{5... | collective-permute-start | bytes 2162696 | tf_op jit(solution)/shard_map/ppermute | solution.py:25
  155.2 0.9 copy-start.2
  156.1 34.4 %collective-permute-start.5 = (bf16[256,1408]{1,0:T(8,128)(2,1)S(1)}, bf16[256,1408]{1,0:T(8,128)(2,1)}, u32[]{:S(2)}, u32[]{:S(2)}) collective-permute-start(bf16[256,1408]{1,0:T(8,128)(2,1)S(1)} %collective-permute-done.4), channel_id=1, source_target_pairs={{0,4},{4,8},{8,12},{12,16},{16,20},{20,24},{24,28},{28,0},{1,5},{5... | collective-permute-start | bytes 2162696 | tf_op jit(solution)/shard_map/ppermute | solution.py:25
  190.4 24.0 %collective-permute-start.6 = (bf16[256,1408]{1,0:T(8,128)(2,1)}, bf16[256,1408]{1,0:T(8,128)(2,1)}, u32[]{:S(2)}, u32[]{:S(2)}) collective-permute-start(bf16[256,1408]{1,0:T(8,128)(2,1)} %collective-permute-done.5), channel_id=1, source_target_pairs={{0,4},{4,8},{8,12},{12,16},{16,20},{20,24},{24,28},{28,0},{1,5},{5... | collective-permute-start | bytes 2162696 | tf_op jit(solution)/shard_map/ppermute | solution.py:25
  216.8 5.4 %copy-start.3 = (bf16[256,1408]{1,0:T(8,128)(2,1)S(1)}, bf16[256,1408]{1,0:T(8,128)(2,1)}, u32[]{:S(2)}) copy-start(bf16[256,1408]{1,0:T(8,128)(2,1)} %copy-done.2) | copy-start | bytes 2162692
  218.1 4.2 %copy-start.1 = (bf16[256,1408]{1,0:T(8,128)(2,1)S(1)}, bf16[256,1408]{1,0:T(8,128)(2,1)}, u32[]{:S(2)}) copy-start(bf16[256,1408]{1,0:T(8,128)(2,1)} %copy-done) | copy-start | bytes 2162692
Sparse Core Ops, SparseCore 0:
  10.9 31.2 all-gather.3
  45.0 131.8 all-gather.5
  179.7 106.3 all-gather.7
  302.9 36.0 reduce-scatter.1
